TPU v7x, 32 devices: a whole 2x2x4 slice. The times are simulated.
32 devices in a mesh: grp: 2 (over y), kv: 4 (over z), tp: 4 (over x, core).
Axes of the slice: x: 2, y: 2, z: 4, core: 2. Of those that a mesh axis runs over, the one named last changes fastest.
Arguments:
- stream_in: bfloat16 [96, 4096], P(('grp', 'tp'), 'kv'), parts along dimension 0, may hold values from -40 to 40
- positions: int32 [96], P(('grp', 'kv')), parts along dimension 0, may hold values from 1024 to 32767
- ret_state: float32 [96, 16, 128, 128], P(('grp', 'kv'), 'tp'), parts along dimension 0, may hold values from -0.6 to 0.6
- first_gain: float32 [4096], P('kv'), may hold values from 0.1 to 1.9
- first_gate: bfloat16 [4096, 11008], P('kv', 'tp'), may hold values from -0.09375 to 0.09375
- first_up: bfloat16 [4096, 11008], P('kv', 'tp'), may hold values from -0.09375 to 0.09375
- first_down: bfloat16 [11008, 4096], P('tp', 'kv'), may hold values from -0.1875 to 0.1875
- mix_gain: float32 [4096], P('kv'), may hold values from 0.1 to 1.9
- w_query: bfloat16 [4096, 2048], P('kv', 'tp'), may hold values from -0.09375 to 0.09375
- w_key: bfloat16 [4096, 2048], P('kv', 'tp'), may hold values from -0.09375 to 0.09375
- w_value: bfloat16 [4096, 2048], P('kv', 'tp'), may hold values from -0.09375 to 0.09375
- w_outgate: bfloat16 [4096, 2048], P('kv', 'tp'), may hold values from -0.09375 to 0.09375
- w_out: bfloat16 [2048, 4096], P('tp', 'kv'), may hold values from -0.21875 to 0.21875
- head_gain: float32 [2048], P('tp'), may hold values from 0.1 to 1.9
- second_gain: float32 [4096], P('kv'), may hold values from 0.1 to 1.9
- second_gate: bfloat16 [4096, 11008], P('kv', 'tp'), may hold values from -0.09375 to 0.09375
- second_up: bfloat16 [4096, 11008], P('kv', 'tp'), may hold values from -0.09375 to 0.09375
- second_down: bfloat16 [11008, 4096], P('tp', 'kv'), may hold values from -0.1875 to 0.1875
Outputs:
- stream_out: bfloat16 [96, 4096], P(('grp', 'tp'), 'kv'), parts along dimension 0
- new_state: float32 [96, 16, 128, 128], P(('grp', 'kv'), 'tp'), parts along dimension 0
There are 2 independent parts, one for each index of `grp`. A program takes and returns all parts, laid end to end along the dimension named above; an argument that names none is the same for every part. Nothing has to cross between parts.
All inputs are finite; a program needn't handle non-finite values.
Results may differ from a plain program's by a relative error of at most 0.03.
Values may be sent and summed in bfloat16 or wider, within the bound.
A program may use at most 128 MiB of HBM per device.

v0:
```python
import jax
import jax.numpy as jnp
from jax import lax
from jax.sharding import PartitionSpec as P

D = 4096
EPS_NORM = 1e-06
EPS_GROUP = 1e-05


def widen_rows(stream_rows):
    return lax.all_gather(stream_rows, "tp", axis=0, tiled=True)


def prepare(stream, norm_gain):
    widened = stream.astype(jnp.float32)
    squares = jnp.sum(widened * widened, axis=1)
    scaled = (widened * norm_gain).astype(jnp.bfloat16)
    return (squares, scaled)


def feed_forward(stream, norm_gain, w_gate, w_up):
    squares, scaled = prepare(stream, norm_gain)
    gate_part = jnp.dot(scaled, w_gate, preferred_element_type=jnp.float32)
    up_part = jnp.dot(scaled, w_up, preferred_element_type=jnp.float32)
    gate_part, up_part, squares = (
        lax.psum(gate_part.astype(jnp.bfloat16), "kv").astype(jnp.float32),
        lax.psum(up_part.astype(jnp.bfloat16), "kv").astype(jnp.float32),
        lax.psum(squares.astype(jnp.bfloat16), "kv").astype(jnp.float32),
    )
    factor = lax.rsqrt(squares / D + EPS_NORM)[:, None]
    return (jax.nn.silu(factor * gate_part) * (factor * up_part)).astype(jnp.bfloat16)


def advance(stream, inputs_back, weight_back, factor_branch):
    row_count = stream.shape[0] // lax.axis_size("tp")
    row_share = lax.psum_scatter(
        jnp.dot(inputs_back, weight_back, preferred_element_type=jnp.float32).astype(jnp.bfloat16),
        "tp",
        scatter_dimension=0,
        tiled=True,
    ).astype(jnp.float32)
    own_rows = lax.dynamic_slice_in_dim(stream, lax.axis_index("tp") * row_count, row_count, 0)
    return (own_rows.astype(jnp.float32) + factor_branch * row_share).astype(jnp.bfloat16)


def rotate(values_in, cosine, sine_part):
    half_dim = values_in.shape[-1] // 2
    lower_half = values_in[..., :half_dim]
    upper_half = values_in[..., half_dim:]
    return jnp.concatenate(
        [
            lower_half * cosine - upper_half * sine_part,
            lower_half * sine_part + upper_half * cosine,
        ],
        axis=-1,
    )


def retention(
    stream, norm_gain, w_query, w_key, w_value, w_outgate, head_gain, state_old, positions
):
    squares, scaled = prepare(stream, norm_gain)
    query_part = jnp.dot(scaled, w_query, preferred_element_type=jnp.float32)
    key_part = jnp.dot(scaled, w_key, preferred_element_type=jnp.float32)
    value_part = jnp.dot(scaled, w_value, preferred_element_type=jnp.float32)
    gate_part = jnp.dot(scaled, w_outgate, preferred_element_type=jnp.float32)
    query_part, key_part, value_part, gate_part, squares = (
        lax.psum_scatter(
            query_part.astype(jnp.bfloat16), "kv", scatter_dimension=0, tiled=True
        ).astype(jnp.float32),
        lax.psum_scatter(
            key_part.astype(jnp.bfloat16), "kv", scatter_dimension=0, tiled=True
        ).astype(jnp.float32),
        lax.psum_scatter(
            value_part.astype(jnp.bfloat16), "kv", scatter_dimension=0, tiled=True
        ).astype(jnp.float32),
        lax.psum_scatter(
            gate_part.astype(jnp.bfloat16), "kv", scatter_dimension=0, tiled=True
        ).astype(jnp.float32),
        lax.psum_scatter(
            squares.astype(jnp.bfloat16), "kv", scatter_dimension=0, tiled=True
        ).astype(jnp.float32),
    )
    factor = lax.rsqrt(squares / D + EPS_NORM)[:, None]
    sequences = state_old.shape[0]
    head_count = state_old.shape[1]
    width_head = state_old.shape[2]
    shape_heads = (sequences, head_count, width_head)
    queries = (factor * query_part).reshape(shape_heads)
    key_vec = (factor * key_part).reshape(shape_heads)
    values_new = (factor * value_part).reshape(shape_heads)
    gate_pre = (factor * gate_part).reshape(shape_heads)
    half_dim = width_head // 2
    inverse = 10000.0 ** (-jnp.arange(half_dim, dtype=jnp.float32) / half_dim)
    angles = positions.astype(jnp.float32)[:, None] * inverse[None, :]
    cosine = jnp.cos(angles)[:, None, :]
    sine_part = jnp.sin(angles)[:, None, :]
    queries = rotate(queries, cosine, sine_part)
    key_vec = rotate(key_vec, cosine, sine_part) * width_head ** (-0.5)
    head_ids = (lax.axis_index("tp") * head_count + jnp.arange(head_count)).astype(jnp.float32)
    decays = jnp.exp(jnp.log1p(-(2.0 ** (-5.0 - head_ids))))
    carried = jnp.einsum("shd,shde->she", queries, state_old, precision=lax.Precision.HIGHEST)
    within = jnp.sum(queries * key_vec, axis=-1, keepdims=True)
    mixture = decays[None, :, None] * carried + within * values_new
    new_state = (
        decays[None, :, None, None] * state_old + key_vec[..., :, None] * values_new[..., None, :]
    )
    average = jnp.mean(mixture, axis=-1, keepdims=True)
    centered = mixture - average
    variance = jnp.mean(centered * centered, axis=-1, keepdims=True)
    normed = centered * lax.rsqrt(variance + EPS_GROUP) * head_gain.reshape(head_count, width_head)
    ret_out = (
        (jax.nn.silu(gate_pre) * normed)
        .astype(jnp.bfloat16)
        .reshape(sequences, head_count * width_head)
    )
    return (lax.all_gather(ret_out, "kv", axis=0, tiled=True), new_state)


def per_device(
    stream_in,
    positions,
    ret_state,
    first_gain,
    first_gate,
    first_up,
    first_down,
    mix_gain,
    w_query,
    w_key,
    w_value,
    w_outgate,
    w_out,
    head_gain,
    second_gain,
    second_gate,
    second_up,
    second_down,
):
    stream = widen_rows(stream_in)
    hidden = feed_forward(stream, first_gain, first_gate, first_up)
    stream = advance(stream, hidden, first_down, 0.5)
    stream = widen_rows(stream)
    ret_out, new_state = retention(
        stream, mix_gain, w_query, w_key, w_value, w_outgate, head_gain, ret_state, positions
    )
    stream = advance(stream, ret_out, w_out, 1.0)
    stream = widen_rows(stream)
    hidden = feed_forward(stream, second_gain, second_gate, second_up)
    stream = advance(stream, hidden, second_down, 0.5)
    return (stream, new_state)


def solution(mesh):
    in_specs = (
        P(("grp", "tp"), "kv"),
        P(("grp", "kv")),
        P(("grp", "kv"), "tp", None, None),
        P("kv"),
        P("kv", "tp"),
        P("kv", "tp"),
        P("tp", "kv"),
        P("kv"),
        P("kv", "tp"),
        P("kv", "tp"),
        P("kv", "tp"),
        P("kv", "tp"),
        P("tp", "kv"),
        P("tp"),
        P("kv"),
        P("kv", "tp"),
        P("kv", "tp"),
        P("tp", "kv"),
    )
    out_specs = (P(("grp", "tp"), "kv"), P(("grp", "kv"), "tp", None, None))
    return jax.shard_map(
        per_device, mesh=mesh, in_specs=in_specs, out_specs=out_specs, check_vma=False
    )
```

profile of v0, /device:TPU:1, one launch (start us, length us, event | category | flops | bytes accessed | tf_op | source)
XLA Modules:
  0.0 235.9 jit_solution(9021519236069175945)
XLA Ops:
  7.2 0.0 copy-start
  7.2 0.0 all-reduce.23.cloned.1.call-start
  7.2 6.7 %all-gather = bf16[4,12,1024]{2,1,0:T(8,128)(2,1)S(1)} all-gather(bf16[1,12,1024]{2,1,0:T(8,128)(2,1)} %bitcast.43), channel_id=1, replica_groups=mesh['grp'=2,'kv'=4,'tp'=4] {'tp'}, dimensions={0}, use_global_device_ids=true | all-gather | bytes 122880 | tf_op jit(solution)/shard_map/all_gather | solution.py:12
  14.0 0.0 copy-start.1
  14.0 0.0 copy-start.10
  14.0 5.3 %convolution_convert_fusion.2 = bf16[48,2752]{1,0:T(8,128)(2,1)} fusion(bf16[1024,2752]{0,1:T(8,128)(2,1)} %param.23, bf16[48,1024]{1,0:T(8,128)(2,1)S(1)} %reshape.132, f32[1024]{0:T(1024)} %param.21), kind=kOutput, calls=%fused_computation.3 | convolution fusion | flops 270812160 | bytes 6002688 | tf_op jit(solution)/shard_map/dot_general | solution.py:25
  19.3 0.0 copy-start.8
  19.3 2.5 %convolution_convert_fusion.3 = bf16[48,2752]{1,0:T(8,128)(2,1)} fusion(bf16[1024,2752]{0,1:T(8,128)(2,1)S(1)} %copy-done.1, bf16[48,1024]{1,0:T(8,128)(2,1)S(1)} %reshape.132, f32[1024]{0:T(1024)S(1)} %copy-done.5), kind=kOutput, calls=%fused_computation.4 | convolution fusion | flops 270812160 | bytes 6002688 | tf_op jit(solution)/shard_map/dot_general | solution.py:24
  21.8 0.0 all-reduce.23.cloned.1.call-update
  21.8 0.0 all-reduce.21.cloned.1.call-start
  21.9 0.1 fusion.14
  22.0 10.6 %psum.42 = bf16[48]{0:T(256)(128)(2,1)S(1)} all-reduce(bf16[48]{0:T(256)(128)(2,1)S(1)} %fusion.14), channel_id=1, replica_groups=mesh['grp'=2,'kv'=4,'tp'=4] {'kv'}, use_global_device_ids=true, to_apply=%region_1.0 | all-reduce | flops 48 | bytes 192 | tf_op jit(solution)/shard_map/psum | solution.py:29
  32.6 0.1 multiply_cosine_fusion
  32.7 28.6 %all-reduce.23.cloned.1.call-done = (bf16[48,2752]{1,0:T(8,128)(2,1)}, bf16[48,2752]{1,0:T(8,128)(2,1)}) async-done(((bf16[48,2752]{1,0:T(8,128)(2,1)}, bf16[48,2752]{1,0:T(8,128)(2,1)}), (bf16[48,2752]{1,0:T(8,128)(2,1)}, bf16[48,2752]{1,0:T(8,128)(2,1)})) %all-reduce.23.cloned.1.call-update) | async-done | bytes 528400 | tf_op jit(solution)/shard_map/psum | solution.py:28
  61.3 3.9 %convolution_convert_fusion.6 = bf16[48,1024]{1,0:T(8,128)(2,1)S(1)} fusion(bf16[2752,1024]{1,0:T(8,128)(2,1)} %param.24, bf16[48,2752]{1,0:T(8,128)(2,1)} %get-tuple-element.4, bf16[48,2752]{1,0:T(8,128)(2,1)} %get-tuple-element.5, f32[48]{0:T(128)S(1)} %add_rsqrt_fusion.2), kind=kOutput, calls=%fused_computation.8 | convolution fusion | flops 271902720 | bytes 6262976 | tf_op jit(solution)/shard_map/dot_general | solution.py:38
  65.3 7.6 %fusion = bf16[16,1024]{1,0:T(8,128)(2,1)S(1)} fusion(bf16[48,1024]{1,0:T(8,128)(2,1)S(1)} %convolution_convert_fusion.6), kind=kCustom, calls=%all-reduce-scatter | all-reduce-scatter fusion | flops 65537 | bytes 131584
  72.9 4.2 %collective-permute-start = (bf16[12,1024]{1,0:T(8,128)(2,1)S(1)}, bf16[12,1024]{1,0:T(8,128)(2,1)S(1)}, u32[]{:S(2)}, u32[]{:S(2)}) collective-permute-start(bf16[12,1024]{1,0:T(8,128)(2,1)S(1)} %slice.20), channel_id=1, source_target_pairs={{0,1},{1,2},{2,3},{4,5},{5,6},{6,7},{8,9},{9,10},{10,11},{12,13},{... | collective-permute-start | bytes 73736
  77.1 0.6 dynamic-slice.18
  78.4 0.6 fusion.39
  80.3 0.2 concatenate.12
  80.5 4.3 %all-gather.1 = bf16[4,12,1024]{2,1,0:T(8,128)(2,1)S(1)} all-gather(bf16[1,12,1024]{2,1,0:T(8,128)(2,1)S(1)} %fusion.28), channel_id=1, replica_groups=mesh['grp'=2,'kv'=4,'tp'=4] {'tp'}, dimensions={0}, use_global_device_ids=true | all-gather | bytes 122880 | tf_op jit(solution)/shard_map/all_gather | solution.py:12
  84.8 0.1 fusion.16
  84.9 8.9 %all-reduce.1 = bf16[48]{0:T(256)(128)(2,1)S(1)} all-reduce(bf16[48]{0:T(256)(128)(2,1)S(1)} %fusion.16), channel_id=3, replica_groups=mesh['grp'=2,'kv'=4,'tp'=4] {'kv'}, use_global_device_ids=true, to_apply=%region_6.7.clone | all-reduce | flops 48 | bytes 192
  93.8 0.3 convolution_convert_fusion.9
  94.1 0.3 convolution_convert_fusion.8
  94.4 1.5 convolution_convert_fusion.7
  95.9 1.5 convolution_convert_fusion.10
  97.4 10.5 %fusion.38 = (bf16[16,512]{1,0:T(8,128)(2,1)S(1)}, bf16[16,512]{1,0:T(8,128)(2,1)S(1)}, bf16[16,512]{1,0:T(8,128)(2,1)S(1)}, bf16[16,512]{1,0:T(8,128)(2,1)S(1)}) fusion(bf16[48,512]{1,0:T(8,128)(2,1)S(1)} %convolution_convert_fusion.10, bf16[48,512]{1,0:T(8,128)(2,1)S(1)} %convolution_convert_fusion.7, bf16[48,512]{1,0:T(8,128)(2,1)S(1)} %convolution_convert_fusion.9, ...), kind=kCustom, calls=%all-reduce-scatter.7 | all-reduce-scatter fusion | flops 131073 | bytes 262656
  108.0 1.6 collective-permute-start.3
  109.6 1.9 collective-permute-start.2
  111.5 3.3 %collective-permute-start.4 = (bf16[12,512]{1,0:T(8,128)(2,1)S(1)}, bf16[12,512]{1,0:T(8,128)(2,1)S(1)}, u32[]{:S(2)}, u32[]{:S(2)}) collective-permute-start(bf16[12,512]{1,0:T(8,128)(2,1)S(1)} %slice.24), channel_id=1, source_target_pairs={{0,4},{4,8},{8,12},{1,5},{5,9},{9,13},{2,6},{6,10},{10,14},{3,7},{... | collective-permute-start | bytes 36872
  114.8 1.9 collective-permute-start.1
  116.8 0.1 fusion.35
  116.9 0.1 concatenate.15
  117.0 0.2 concatenate.14
  117.2 0.2 concatenate.16
  117.4 0.3 collective-permute-done.1
  117.6 0.1 concatenate.13
  117.7 0.1 convert_multiply_fusion.7
  117.9 0.1 multiply_subtract_fusion
  118.0 0.1 pad_maximum_fusion
  118.1 4.6 %fusion.41 = f32[12,4,1,128]{3,2,1,0:T(1,128)S(1)} fusion(f32[12,4,128,1]{2,3,1,0:T(1,128)S(1)} %bitcast.42, f32[12,4,128,128]{3,2,1,0:T(8,128)} %param.20), kind=kOutput, calls=%fused_computation.70 | convolution fusion | flops 9437184 | bytes 3194880 | tf_op jit(solution)/shard_map/shd,shde->she/dot_general | solution.py:103
  122.7 0.2 fusion.40
  122.9 0.2 multiply_reduce_fusion
  123.1 0.1 fusion.31
  123.2 10.3 %all-gather.2 = bf16[4,12,512]{2,1,0:T(8,128)(2,1)S(1)} all-gather(bf16[1,12,512]{2,1,0:T(8,128)(2,1)S(1)} %reshape.135), channel_id=1, replica_groups=mesh['grp'=2,'kv'=4,'tp'=4] {'kv'}, dimensions={0}, use_global_device_ids=true | all-gather | bytes 61440 | tf_op jit(solution)/shard_map/all_gather | solution.py:118
  133.5 0.3 convolution_convert_fusion.5
  133.8 15.0 %fusion.5 = bf16[16,1024]{1,0:T(8,128)(2,1)S(1)} fusion(bf16[48,1024]{1,0:T(8,128)(2,1)S(1)} %convolution_convert_fusion.5), kind=kCustom, calls=%all-reduce-scatter.5 | all-reduce-scatter fusion | flops 65537 | bytes 131584
  148.8 4.2 %collective-permute-start.5 = (bf16[12,1024]{1,0:T(8,128)(2,1)S(1)}, bf16[12,1024]{1,0:T(8,128)(2,1)S(1)}, u32[]{:S(2)}, u32[]{:S(2)}) collective-permute-start(bf16[12,1024]{1,0:T(8,128)(2,1)S(1)} %slice.25), channel_id=1, source_target_pairs={{0,1},{1,2},{2,3},{4,5},{5,6},{6,7},{8,9},{9,10},{10,11},{12,13},{... | collective-permute-start | bytes 73736
  153.1 1.0 collective-permute-done.5
  154.1 0.1 concatenate.17
  154.2 6.3 %all-gather.3 = bf16[4,12,1024]{2,1,0:T(8,128)(2,1)S(1)} all-gather(bf16[1,12,1024]{2,1,0:T(8,128)(2,1)S(1)} %fusion.29), channel_id=1, replica_groups=mesh['grp'=2,'kv'=4,'tp'=4] {'tp'}, dimensions={0}, use_global_device_ids=true | all-gather | bytes 122880 | tf_op jit(solution)/shard_map/all_gather | solution.py:12
  160.6 5.1 %convolution_convert_fusion = bf16[48,2752]{1,0:T(8,128)(2,1)} fusion(bf16[1024,2752]{0,1:T(8,128)(2,1)} %param.34, bf16[48,1024]{1,0:T(8,128)(2,1)S(1)} %reshape.138, f32[1024]{0:T(1024)S(1)} %copy-done.6), kind=kOutput, calls=%fused_computation.1 | convolution fusion | flops 270812160 | bytes 6002688 | tf_op jit(solution)/shard_map/dot_general | solution.py:25
  165.7 5.1 %convolution_convert_fusion.1 = bf16[48,2752]{1,0:T(8,128)(2,1)} fusion(bf16[1024,2752]{0,1:T(8,128)(2,1)} %param.33, bf16[48,1024]{1,0:T(8,128)(2,1)S(1)} %reshape.138, f32[1024]{0:T(1024)S(1)} %copy-done.6), kind=kOutput, calls=%fused_computation.2 | convolution fusion | flops 270812160 | bytes 6002688 | tf_op jit(solution)/shard_map/dot_general | solution.py:24
  170.8 0.0 all-reduce.21.cloned.1.call-update
  170.8 0.1 fusion.18
  170.9 8.8 %psum.45 = bf16[48]{0:T(256)(128)(2,1)S(1)} all-reduce(bf16[48]{0:T(256)(128)(2,1)S(1)} %fusion.18), channel_id=1, replica_groups=mesh['grp'=2,'kv'=4,'tp'=4] {'kv'}, use_global_device_ids=true, to_apply=%region_16.17 | all-reduce | flops 48 | bytes 192 | tf_op jit(solution)/shard_map/psum | solution.py:29
  179.8 29.1 %all-reduce.21.cloned.1.call-done = (bf16[48,2752]{1,0:T(8,128)(2,1)}, bf16[48,2752]{1,0:T(8,128)(2,1)}) async-done(((bf16[48,2752]{1,0:T(8,128)(2,1)}, bf16[48,2752]{1,0:T(8,128)(2,1)}), (bf16[48,2752]{1,0:T(8,128)(2,1)}, bf16[48,2752]{1,0:T(8,128)(2,1)})) %all-reduce.21.cloned.1.call-update) | async-done | bytes 528400 | tf_op jit(solution)/shard_map/psum | solution.py:28
  208.9 3.9 %convolution_convert_fusion.4 = bf16[48,1024]{1,0:T(8,128)(2,1)S(1)} fusion(bf16[2752,1024]{1,0:T(8,128)(2,1)} %param.35, bf16[48,2752]{1,0:T(8,128)(2,1)} %get-tuple-element.2, bf16[48,2752]{1,0:T(8,128)(2,1)} %get-tuple-element.3, f32[48]{0:T(128)S(1)} %add_rsqrt_fusion.1), kind=kOutput, calls=%fused_computation.6 | convolution fusion | flops 271902720 | bytes 6262976 | tf_op jit(solution)/shard_map/dot_general | solution.py:38
  212.9 7.6 %fusion.6 = bf16[16,1024]{1,0:T(8,128)(2,1)S(1)} fusion(bf16[48,1024]{1,0:T(8,128)(2,1)S(1)} %convolution_convert_fusion.4), kind=kCustom, calls=%all-reduce-scatter.6 | all-reduce-scatter fusion | flops 65537 | bytes 131584
  220.5 4.2 %collective-permute-start.6 = (bf16[12,1024]{1,0:T(8,128)(2,1)S(1)}, bf16[12,1024]{1,0:T(8,128)(2,1)S(1)}, u32[]{:S(2)}, u32[]{:S(2)}) collective-permute-start(bf16[12,1024]{1,0:T(8,128)(2,1)S(1)} %slice.26), channel_id=1, source_target_pairs={{0,1},{1,2},{2,3},{4,5},{5,6},{6,7},{8,9},{9,10},{10,11},{12,13},{... | collective-permute-start | bytes 73736
  224.7 3.6 %multiply_add_fusion = f32[12,4,128,128]{3,2,1,0:T(8,128)} fusion(f32[12,4,128,128]{3,2,1,0:T(8,128)} %param.20, f32[12,4,128]{2,1,0:T(4,128)S(1)} %reshape.129, f32[12,4,128]{2,1,0:T(4,128)S(1)} %get-tuple-element.31, f32[4]{0:T(128)S(1)} %log-plus-one_exponential_fusion), kind=kLoop, calls=%fused_computation.5 | loop fusion | flops 2359296 | bytes 6340624 | tf_op jit(solution)/shard_map/add | solution.py:107
  228.3 0.2 concatenate.18
  228.4 0.7 add_convert_fusion
  (48 shorter events, 0.4 us)
Async XLA Ops:
  7.2 126.4 %copy-start = (bf16[512,1024]{1,0:T(8,128)(2,1)S(1)}, bf16[512,1024]{1,0:T(8,128)(2,1)}, u32[]{:S(2)}) copy-start(bf16[512,1024]{1,0:T(8,128)(2,1)} %param.30) | copy-start | bytes 3145732
  7.2 12.1 %copy-start.5 = (f32[1024]{0:T(1024)S(1)}, f32[1024]{0:T(1024)}, u32[]{:S(2)}) copy-start(f32[1024]{0:T(1024)} %param.21) | copy-start | bytes 12292
  7.2 54.1 %all-reduce.23.cloned.1.call-start = ((), (), s32[]{:S(2)}) async-start(), calls=%async_computation.1 | async-start | bytes 1081344 | tf_op jit(solution)/shard_map/psum | solution.py:28
  14.0 5.3 %copy-start.1 = (bf16[1024,2752]{0,1:T(8,128)(2,1)S(1)}, bf16[1024,2752]{0,1:T(8,128)(2,1)}, u32[]{:S(2)}) copy-start(bf16[1024,2752]{0,1:T(8,128)(2,1)} %param.22) | copy-start | bytes 16908292
  14.0 8.0 %copy-start.10 = (s32[12]{0:T(128)S(1)}, s32[12]{0:T(128)}, u32[]{:S(2)}) copy-start(s32[12]{0:T(128)} %param.19) | copy-start | bytes 148
  19.3 57.9 %copy-start.9 = (u32[32]{0:T(128)S(1)}, u32[32]{0:T(128)}, u32[]{:S(2)}) copy-start(u32[32]{0:T(128)} %constant.53) | copy-start | bytes 388
  19.3 59.1 %copy-start.8 = (u32[32]{0:T(128)S(1)}, u32[32]{0:T(128)}, u32[]{:S(2)}) copy-start(u32[32]{0:T(128)} %constant.57) | copy-start | bytes 388
  21.8 72.0 %copy-start.2 = (bf16[1024,512]{1,0:T(8,128)(2,1)S(1)}, bf16[1024,512]{1,0:T(8,128)(2,1)}, u32[]{:S(2)}) copy-start(bf16[1024,512]{1,0:T(8,128)(2,1)} %param.26) | copy-start | bytes 3145732
  21.8 72.0 %copy-start.4 = (f32[1024]{0:T(1024)S(1)}, f32[1024]{0:T(1024)}, u32[]{:S(2)}) copy-start(f32[1024]{0:T(1024)} %param.25) | copy-start | bytes 12292
  21.8 72.3 %copy-start.3 = (bf16[1024,512]{1,0:T(8,128)(2,1)S(1)}, bf16[1024,512]{1,0:T(8,128)(2,1)}, u32[]{:S(2)}) copy-start(bf16[1024,512]{1,0:T(8,128)(2,1)} %param.27) | copy-start | bytes 3145732
  21.8 187.1 %all-reduce.21.cloned.1.call-start = ((), (), s32[]{:S(2)}) async-start(), calls=%async_computation | async-start | bytes 1081344 | tf_op jit(solution)/shard_map/psum | solution.py:28
  65.3 57.8 %copy-start.7 = (f32[512]{0:T(512)S(1)}, f32[512]{0:T(512)}, u32[]{:S(2)}) copy-start(f32[512]{0:T(512)} %param.31) | copy-start | bytes 6148
  72.9 7.4 %collective-permute-start = (bf16[12,1024]{1,0:T(8,128)(2,1)S(1)}, bf16[12,1024]{1,0:T(8,128)(2,1)S(1)}, u32[]{:S(2)}, u32[]{:S(2)}) collective-permute-start(bf16[12,1024]{1,0:T(8,128)(2,1)S(1)} %slice.20), channel_id=1, source_target_pairs={{0,1},{1,2},{2,3},{4,5},{5,6},{6,7},{8,9},{9,10},{10,11},{12,13},{... | collective-permute-start | bytes 73736
  94.1 66.5 %copy-start.6 = (f32[1024]{0:T(1024)S(1)}, f32[1024]{0:T(1024)}, u32[]{:S(2)}) copy-start(f32[1024]{0:T(1024)} %param.32) | copy-start | bytes 12292
  108.0 8.9 %collective-permute-start.3 = (bf16[12,512]{1,0:T(8,128)(2,1)S(1)}, bf16[12,512]{1,0:T(8,128)(2,1)S(1)}, u32[]{:S(2)}, u32[]{:S(2)}) collective-permute-start(bf16[12,512]{1,0:T(8,128)(2,1)S(1)} %slice.23), channel_id=1, source_target_pairs={{0,4},{4,8},{8,12},{1,5},{5,9},{9,13},{2,6},{6,10},{10,14},{3,7},{... | collective-permute-start | bytes 36872
  109.6 7.4 %collective-permute-start.2 = (bf16[12,512]{1,0:T(8,128)(2,1)S(1)}, bf16[12,512]{1,0:T(8,128)(2,1)S(1)}, u32[]{:S(2)}, u32[]{:S(2)}) collective-permute-start(bf16[12,512]{1,0:T(8,128)(2,1)S(1)} %slice.22), channel_id=1, source_target_pairs={{0,4},{4,8},{8,12},{1,5},{5,9},{9,13},{2,6},{6,10},{10,14},{3,7},{... | collective-permute-start | bytes 36872
  111.5 5.6 %collective-permute-start.4 = (bf16[12,512]{1,0:T(8,128)(2,1)S(1)}, bf16[12,512]{1,0:T(8,128)(2,1)S(1)}, u32[]{:S(2)}, u32[]{:S(2)}) collective-permute-start(bf16[12,512]{1,0:T(8,128)(2,1)S(1)} %slice.24), channel_id=1, source_target_pairs={{0,4},{4,8},{8,12},{1,5},{5,9},{9,13},{2,6},{6,10},{10,14},{3,7},{... | collective-permute-start | bytes 36872
  114.8 2.8 %collective-permute-start.1 = (bf16[12,512]{1,0:T(8,128)(2,1)S(1)}, bf16[12,512]{1,0:T(8,128)(2,1)S(1)}, u32[]{:S(2)}, u32[]{:S(2)}) collective-permute-start(bf16[12,512]{1,0:T(8,128)(2,1)S(1)} %slice.21), channel_id=1, source_target_pairs={{0,4},{4,8},{8,12},{1,5},{5,9},{9,13},{2,6},{6,10},{10,14},{3,7},{... | collective-permute-start | bytes 36872
  148.8 5.2 %collective-permute-start.5 = (bf16[12,1024]{1,0:T(8,128)(2,1)S(1)}, bf16[12,1024]{1,0:T(8,128)(2,1)S(1)}, u32[]{:S(2)}, u32[]{:S(2)}) collective-permute-start(bf16[12,1024]{1,0:T(8,128)(2,1)S(1)} %slice.25), channel_id=1, source_target_pairs={{0,1},{1,2},{2,3},{4,5},{5,6},{6,7},{8,9},{9,10},{10,11},{12,13},{... | collective-permute-start | bytes 73736
  220.5 7.8 %collective-permute-start.6 = (bf16[12,1024]{1,0:T(8,128)(2,1)S(1)}, bf16[12,1024]{1,0:T(8,128)(2,1)S(1)}, u32[]{:S(2)}, u32[]{:S(2)}) collective-permute-start(bf16[12,1024]{1,0:T(8,128)(2,1)S(1)} %slice.26), channel_id=1, source_target_pairs={{0,1},{1,2},{2,3},{4,5},{5,6},{6,7},{8,9},{9,10},{10,11},{12,13},{... | collective-permute-start | bytes 73736
Sparse Core Ops, SparseCore 0:
  21.9 39.3 all-reduce.22
  170.9 37.9 all-reduce.20
where the time goes:
time: 237 us; the launch traced here: 236 us
  blocking collectives  96.5 us (41%)
  waiting for transfers between devices  59 us (25%)
  matrix products  34.3 us (14%)
  starting transfers between devices  21.4 us (9%)
  between operations  16.5 us (7%)
  other arithmetic  5.63 us (2%)
  local copies, waits for them, and re-layouts  2.53 us (1%)
    psum x2, waiting for transfers between devices, feed_forward(): lax.psum(up_part.astype(jnp.bfloat16), 'kv').astype(jnp.float32)  57.7 us
    unnamed x5, blocking collectives  49.5 us
    unnamed x7, starting transfers between devices  21.3 us
    psum x2, blocking collectives, feed_forward(): lax.psum(squares.astype(jnp.bfloat16), 'kv').astype(jnp.float32)  19.4 us
    all_gather x3, blocking collectives, widen_rows(): return lax.all_gather(stream_rows, 'tp', axis=0, tiled=True)  17.3 us
    dot_general x2, matrix products, feed_forward(): up_part = jnp.dot(scaled, w_up, preferred_element_type=jnp.float32)  10.4 us
    all_gather x1, blocking collectives, retention(): return (lax.all_gather(ret_out, 'kv', axis=0, tiled=True), new_state)  10.3 us
    dot_general x3, matrix products, advance(): jnp.dot(inputs_back, weight_back, preferred_element_type=jnp.float32)  8.18 us
  transfers between devices with their start and end apart: 9, of which 4 were waited for; matrix products, arithmetic and copies ran while one was open for 2% of the time, Pallas kernels for 0%

commit v1 on v0

--- a/solution.py
+++ b/solution.py
@@ -25,7 +25,7 @@
     up_part = jnp.dot(scaled, w_up, preferred_element_type=jnp.float32)
     gate_part, up_part, squares = (
         lax.psum(gate_part.astype(jnp.bfloat16), "kv").astype(jnp.float32),
-        lax.psum(up_part.astype(jnp.bfloat16), "kv").astype(jnp.float32),
+        jnp.sum(lax.all_gather(up_part.astype(jnp.bfloat16), "kv"), axis=0).astype(jnp.float32),
         lax.psum(squares.astype(jnp.bfloat16), "kv").astype(jnp.float32),
     )
     factor = lax.rsqrt(squares / D + EPS_NORM)[:, None]

time: 237 us -> 284 us (1.20)
  waiting for transfers between devices: 59 us -> 97.1 us
  blocking collectives: 96.5 us -> 99.6 us
  matrix products: 34.3 us -> 37.3 us
  other arithmetic: 5.63 us -> 8.48 us
    all_gather x0 -> x2, waiting for transfers between devices: none -> 26.7 us  [feed_forward(): lax.all_gather(up_part.astype(jnp.bfloat16), 'kv')]
    psum x2, waiting for transfers between devices: 57.7 us -> 69.1 us  [feed_forward(): lax.psum(gate_part.astype(jnp.bfloat16), 'kv').astype(jnp.float32)]
    reduce_sum x0 -> x2, other arithmetic: none -> 2.84 us  [feed_forward(): jnp.sum(lax.all_gather(up_part.astype(jnp.bfloat16), 'kv'), axis=0)]
  transfers between devices with their start and end apart: 9 -> 11, of which waited for: 4 -> 6; matrix products, arithmetic and copies ran while one was open for 2% -> 7% of each run, Pallas kernels for 0% -> 0%
where the time goes in v1:
time: 284 us; the launch traced here: 283 us
  blocking collectives  99.6 us (35%)
  waiting for transfers between devices  97.1 us (34%)
  matrix products  37.3 us (13%)
  starting transfers between devices  21.5 us (8%)
  between operations  16.2 us (6%)
  other arithmetic  8.48 us (3%)
    psum x2, waiting for transfers between devices, feed_forward(): lax.psum(gate_part.astype(jnp.bfloat16), 'kv').astype(jnp.float32)  69.1 us
    unnamed x5, blocking collectives  51.9 us
    all_gather x2, waiting for transfers between devices, feed_forward(): lax.all_gather(up_part.astype(jnp.bfloat16), 'kv')  26.7 us
    unnamed x7, starting transfers between devices  21.4 us
    psum x2, blocking collectives, feed_forward(): lax.psum(squares.astype(jnp.bfloat16), 'kv').astype(jnp.float32)  20.1 us
    all_gather x3, blocking collectives, widen_rows(): return lax.all_gather(stream_rows, 'tp', axis=0, tiled=True)  17.4 us
    all_gather x1, blocking collectives, retention(): return (lax.all_gather(ret_out, 'kv', axis=0, tiled=True), new_state)  10.2 us
    dot_general x2, matrix products, feed_forward(): up_part = jnp.dot(scaled, w_up, preferred_element_type=jnp.float32)  10.2 us
  transfers between devices with their start and end apart: 11, of which 6 were waited for; matrix products, arithmetic and copies ran while one was open for 7% of the time, Pallas kernels for 0%

profile of v1, /device:TPU:1, one launch (start us, length us, event | category | flops | bytes accessed | tf_op | source)
XLA Modules:
  0.0 282.8 jit_solution(12755864512717409412)
XLA Ops:
  7.2 0.0 all-gather.9.cloned.1.call-start
  7.2 6.7 %all-gather.2 = bf16[4,12,1024]{2,1,0:T(8,128)(2,1)S(1)} all-gather(bf16[1,12,1024]{2,1,0:T(8,128)(2,1)} %bitcast.47), channel_id=1, replica_groups=mesh['grp'=2,'kv'=4,'tp'=4] {'tp'}, dimensions={0}, use_global_device_ids=true | all-gather | bytes 122880 | tf_op jit(solution)/shard_map/all_gather | solution.py:12
  14.0 5.1 %convolution_convert_fusion.2 = bf16[48,2752]{1,0:T(8,128)(2,1)} fusion(bf16[1024,2752]{0,1:T(8,128)(2,1)} %param.23, bf16[48,1024]{1,0:T(8,128)(2,1)S(1)} %reshape.134, f32[1024]{0:T(1024)} %param.21), kind=kOutput, calls=%fused_computation.3 | convolution fusion | flops 270812160 | bytes 6002688 | tf_op jit(solution)/shard_map/dot_general | solution.py:25
  19.1 0.0 all-reduce.19.cloned.1.call-start
  19.2 5.1 %convolution_convert_fusion.3 = bf16[48,2752]{1,0:T(8,128)(2,1)} fusion(bf16[1024,2752]{0,1:T(8,128)(2,1)} %param.22, bf16[48,1024]{1,0:T(8,128)(2,1)S(1)} %reshape.134, f32[1024]{0:T(1024)S(1)} %copy-done.4), kind=kOutput, calls=%fused_computation.4 | convolution fusion | flops 270812160 | bytes 6002688 | tf_op jit(solution)/shard_map/dot_general | solution.py:24
  24.3 0.0 all-gather.11.cloned.1.call-start
  24.4 0.1 fusion.14
  24.5 11.0 %psum.28 = bf16[48]{0:T(256)(128)(2,1)S(1)} all-reduce(bf16[48]{0:T(256)(128)(2,1)S(1)} %fusion.14), channel_id=1, replica_groups=mesh['grp'=2,'kv'=4,'tp'=4] {'kv'}, use_global_device_ids=true, to_apply=%region_1.0 | all-reduce | flops 48 | bytes 192 | tf_op jit(solution)/shard_map/psum | solution.py:29
  35.5 0.1 multiply_cosine_fusion
  35.7 12.9 %all-gather.9.cloned.1.call-done = bf16[192,2752]{1,0:T(8,128)(2,1)} async-done(((bf16[48,2752]{1,0:T(8,128)(2,1)}), bf16[192,2752]{1,0:T(8,128)(2,1)}) %all-gather.9.cloned.1.call-update) | async-done | bytes 1056784 | tf_op jit(solution)/shard_map/all_gather | solution.py:28
  48.6 1.4 reduce_sum.79
  50.0 34.7 %all-reduce.19.cloned.1.call-done = bf16[48,2752]{1,0:T(8,128)(2,1)} async-done(((bf16[48,2752]{1,0:T(8,128)(2,1)}), bf16[48,2752]{1,0:T(8,128)(2,1)}) %all-reduce.19.cloned.1.call-update) | async-done | bytes 264208 | tf_op jit(solution)/shard_map/psum | solution.py:27
  84.7 4.5 %convolution_convert_fusion.6 = bf16[48,1024]{1,0:T(8,128)(2,1)} fusion(bf16[2752,1024]{1,0:T(8,128)(2,1)} %param.24, bf16[48,2752]{1,0:T(8,128)(2,1)S(1)} %reduce_sum.79, bf16[48,2752]{1,0:T(8,128)(2,1)} %all-reduce.19.cloned.1.call-done, f32[48]{0:T(128)S(1)} %add_rsqrt_fusion.2), kind=kOutput, calls=%fused_computation.8 | convolution fusion | flops 271902720 | bytes 6262976 | tf_op jit(solution)/shard_map/dot_general | solution.py:38
  89.2 9.1 %fusion = bf16[16,1024]{1,0:T(8,128)(2,1)S(1)} fusion(bf16[48,1024]{1,0:T(8,128)(2,1)} %convolution_convert_fusion.6), kind=kCustom, calls=%all-reduce-scatter | all-reduce-scatter fusion | flops 65537 | bytes 131584
  98.3 4.2 %collective-permute-start = (bf16[12,1024]{1,0:T(8,128)(2,1)S(1)}, bf16[12,1024]{1,0:T(8,128)(2,1)S(1)}, u32[]{:S(2)}, u32[]{:S(2)}) collective-permute-start(bf16[12,1024]{1,0:T(8,128)(2,1)S(1)} %slice.20), channel_id=1, source_target_pairs={{0,1},{1,2},{2,3},{4,5},{5,6},{6,7},{8,9},{9,10},{10,11},{12,13},{... | collective-permute-start | bytes 73736
  102.5 0.6 dynamic-slice.18
  103.8 0.6 fusion.39
  105.7 0.2 concatenate.12
  105.9 4.4 %all-gather.3 = bf16[4,12,1024]{2,1,0:T(8,128)(2,1)S(1)} all-gather(bf16[1,12,1024]{2,1,0:T(8,128)(2,1)S(1)} %fusion.28), channel_id=1, replica_groups=mesh['grp'=2,'kv'=4,'tp'=4] {'tp'}, dimensions={0}, use_global_device_ids=true | all-gather | bytes 122880 | tf_op jit(solution)/shard_map/all_gather | solution.py:12
  110.3 0.1 fusion.16
  110.4 9.0 %all-reduce.1 = bf16[48]{0:T(256)(128)(2,1)S(1)} all-reduce(bf16[48]{0:T(256)(128)(2,1)S(1)} %fusion.16), channel_id=5, replica_groups=mesh['grp'=2,'kv'=4,'tp'=4] {'kv'}, use_global_device_ids=true, to_apply=%region_6.7.clone | all-reduce | flops 48 | bytes 192
  119.4 0.3 convolution_convert_fusion.9
  119.7 0.3 convolution_convert_fusion.8
  120.0 1.5 convolution_convert_fusion.7
  121.5 1.5 convolution_convert_fusion.10
  123.0 10.4 %fusion.38 = (bf16[16,512]{1,0:T(8,128)(2,1)S(1)}, bf16[16,512]{1,0:T(8,128)(2,1)S(1)}, bf16[16,512]{1,0:T(8,128)(2,1)S(1)}, bf16[16,512]{1,0:T(8,128)(2,1)S(1)}) fusion(bf16[48,512]{1,0:T(8,128)(2,1)S(1)} %convolution_convert_fusion.10, bf16[48,512]{1,0:T(8,128)(2,1)S(1)} %convolution_convert_fusion.7, bf16[48,512]{1,0:T(8,128)(2,1)S(1)} %convolution_convert_fusion.9, ...), kind=kCustom, calls=%all-reduce-scatter.7 | all-reduce-scatter fusion | flops 131073 | bytes 262656
  133.6 1.7 collective-permute-start.3
  135.2 1.9 collective-permute-start.2
  137.2 3.3 %collective-permute-start.4 = (bf16[12,512]{1,0:T(8,128)(2,1)S(1)}, bf16[12,512]{1,0:T(8,128)(2,1)S(1)}, u32[]{:S(2)}, u32[]{:S(2)}) collective-permute-start(bf16[12,512]{1,0:T(8,128)(2,1)S(1)} %slice.24), channel_id=1, source_target_pairs={{0,4},{4,8},{8,12},{1,5},{5,9},{9,13},{2,6},{6,10},{10,14},{3,7},{... | collective-permute-start | bytes 36872
  140.4 1.9 collective-permute-start.1
  142.4 0.1 fusion.35
  142.5 0.1 concatenate.15
  142.6 0.2 concatenate.14
  142.8 0.2 concatenate.16
  143.0 0.3 collective-permute-done.1
  143.2 0.1 concatenate.13
  143.3 0.1 convert_multiply_fusion.7
  143.5 0.1 multiply_subtract_fusion
  143.6 0.1 pad_maximum_fusion
  143.7 4.6 %fusion.41 = f32[12,4,1,128]{3,2,1,0:T(1,128)S(1)} fusion(f32[12,4,128,1]{2,3,1,0:T(1,128)S(1)} %bitcast.46, f32[12,4,128,128]{3,2,1,0:T(8,128)} %param.20), kind=kOutput, calls=%fused_computation.70 | convolution fusion | flops 9437184 | bytes 3194880 | tf_op jit(solution)/shard_map/shd,shde->she/dot_general | solution.py:103
  148.3 0.2 fusion.40
  148.5 0.2 multiply_reduce_fusion
  148.7 0.1 fusion.31
  148.8 10.2 %all-gather.4 = bf16[4,12,512]{2,1,0:T(8,128)(2,1)S(1)} all-gather(bf16[1,12,512]{2,1,0:T(8,128)(2,1)S(1)} %reshape.137), channel_id=1, replica_groups=mesh['grp'=2,'kv'=4,'tp'=4] {'kv'}, dimensions={0}, use_global_device_ids=true | all-gather | bytes 61440 | tf_op jit(solution)/shard_map/all_gather | solution.py:118
  159.1 0.3 convolution_convert_fusion.5
  159.4 15.0 %fusion.5 = bf16[16,1024]{1,0:T(8,128)(2,1)S(1)} fusion(bf16[48,1024]{1,0:T(8,128)(2,1)S(1)} %convolution_convert_fusion.5), kind=kCustom, calls=%all-reduce-scatter.5 | all-reduce-scatter fusion | flops 65537 | bytes 131584
  174.5 4.2 %collective-permute-start.5 = (bf16[12,1024]{1,0:T(8,128)(2,1)S(1)}, bf16[12,1024]{1,0:T(8,128)(2,1)S(1)}, u32[]{:S(2)}, u32[]{:S(2)}) collective-permute-start(bf16[12,1024]{1,0:T(8,128)(2,1)S(1)} %slice.25), channel_id=1, source_target_pairs={{0,1},{1,2},{2,3},{4,5},{5,6},{6,7},{8,9},{9,10},{10,11},{12,13},{... | collective-permute-start | bytes 73736
  178.7 1.0 collective-permute-done.5
  179.7 0.1 concatenate.17
  179.8 6.3 %all-gather.5 = bf16[4,12,1024]{2,1,0:T(8,128)(2,1)S(1)} all-gather(bf16[1,12,1024]{2,1,0:T(8,128)(2,1)S(1)} %fusion.29), channel_id=1, replica_groups=mesh['grp'=2,'kv'=4,'tp'=4] {'tp'}, dimensions={0}, use_global_device_ids=true | all-gather | bytes 122880 | tf_op jit(solution)/shard_map/all_gather | solution.py:12
  186.2 5.1 %convolution_convert_fusion = bf16[48,2752]{1,0:T(8,128)(2,1)} fusion(bf16[1024,2752]{0,1:T(8,128)(2,1)} %param.34, bf16[48,1024]{1,0:T(8,128)(2,1)S(1)} %reshape.140, f32[1024]{0:T(1024)S(1)} %copy-done.5), kind=kOutput, calls=%fused_computation.1 | convolution fusion | flops 270812160 | bytes 6002688 | tf_op jit(solution)/shard_map/dot_general | solution.py:25
  191.3 0.0 all-reduce.21.cloned.1.call-start
  191.3 5.1 %convolution_convert_fusion.1 = bf16[48,2752]{1,0:T(8,128)(2,1)} fusion(bf16[1024,2752]{0,1:T(8,128)(2,1)} %param.33, bf16[48,1024]{1,0:T(8,128)(2,1)S(1)} %reshape.140, f32[1024]{0:T(1024)S(1)} %copy-done.5), kind=kOutput, calls=%fused_computation.2 | convolution fusion | flops 270812160 | bytes 6002688 | tf_op jit(solution)/shard_map/dot_general | solution.py:24
  196.5 0.1 fusion.18
  196.6 9.1 %psum.30 = bf16[48]{0:T(256)(128)(2,1)S(1)} all-reduce(bf16[48]{0:T(256)(128)(2,1)S(1)} %fusion.18), channel_id=1, replica_groups=mesh['grp'=2,'kv'=4,'tp'=4] {'kv'}, use_global_device_ids=true, to_apply=%region_16.17 | all-reduce | flops 48 | bytes 192 | tf_op jit(solution)/shard_map/psum | solution.py:29
  205.7 13.8 %all-gather.11.cloned.1.call-done = bf16[192,2752]{1,0:T(8,128)(2,1)} async-done(((bf16[48,2752]{1,0:T(8,128)(2,1)}), bf16[192,2752]{1,0:T(8,128)(2,1)}) %all-gather.11.cloned.1.call-update) | async-done | bytes 1056784 | tf_op jit(solution)/shard_map/all_gather | solution.py:28
  219.5 1.4 reduce_sum.85
  220.9 34.4 %all-reduce.21.cloned.1.call-done = bf16[48,2752]{1,0:T(8,128)(2,1)} async-done(((bf16[48,2752]{1,0:T(8,128)(2,1)}), bf16[48,2752]{1,0:T(8,128)(2,1)}) %all-reduce.21.cloned.1.call-update) | async-done | bytes 264208 | tf_op jit(solution)/shard_map/psum | solution.py:27
  255.3 3.9 %convolution_convert_fusion.4 = bf16[48,1024]{1,0:T(8,128)(2,1)S(1)} fusion(bf16[2752,1024]{1,0:T(8,128)(2,1)} %param.35, bf16[48,2752]{1,0:T(8,128)(2,1)S(1)} %reduce_sum.85, bf16[48,2752]{1,0:T(8,128)(2,1)} %all-reduce.21.cloned.1.call-done, f32[48]{0:T(128)S(1)} %add_rsqrt_fusion.1), kind=kOutput, calls=%fused_computation.6 | convolution fusion | flops 271902720 | bytes 6262976 | tf_op jit(solution)/shard_map/dot_general | solution.py:38
  259.2 8.5 %fusion.6 = bf16[16,1024]{1,0:T(8,128)(2,1)S(1)} fusion(bf16[48,1024]{1,0:T(8,128)(2,1)S(1)} %convolution_convert_fusion.4), kind=kCustom, calls=%all-reduce-scatter.6 | all-reduce-scatter fusion | flops 65537 | bytes 131584
  267.6 4.2 %collective-permute-start.6 = (bf16[12,1024]{1,0:T(8,128)(2,1)S(1)}, bf16[12,1024]{1,0:T(8,128)(2,1)S(1)}, u32[]{:S(2)}, u32[]{:S(2)}) collective-permute-start(bf16[12,1024]{1,0:T(8,128)(2,1)S(1)} %slice.26), channel_id=1, source_target_pairs={{0,1},{1,2},{2,3},{4,5},{5,6},{6,7},{8,9},{9,10},{10,11},{12,13},{... | collective-permute-start | bytes 73736
  271.8 3.6 %multiply_add_fusion = f32[12,4,128,128]{3,2,1,0:T(8,128)} fusion(f32[12,4,128,128]{3,2,1,0:T(8,128)} %param.20, f32[12,4,128]{2,1,0:T(4,128)S(1)} %reshape.129, f32[12,4,128]{2,1,0:T(4,128)S(1)} %get-tuple-element.27, f32[4]{0:T(128)S(1)} %log-plus-one_exponential_fusion), kind=kLoop, calls=%fused_computation.5 | loop fusion | flops 2359296 | bytes 6340624 | tf_op jit(solution)/shard_map/add | solution.py:107
  275.4 0.2 concatenate.18
  275.6 0.7 add_convert_fusion
  (54 shorter events, 0.5 us)
Async XLA Ops:
  7.2 151.9 %copy-start = (bf16[512,1024]{1,0:T(8,128)(2,1)S(1)}, bf16[512,1024]{1,0:T(8,128)(2,1)}, u32[]{:S(2)}) copy-start(bf16[512,1024]{1,0:T(8,128)(2,1)} %param.30) | copy-start | bytes 3145732
  7.2 12.0 %copy-start.4 = (f32[1024]{0:T(1024)S(1)}, f32[1024]{0:T(1024)}, u32[]{:S(2)}) copy-start(f32[1024]{0:T(1024)} %param.21) | copy-start | bytes 12292
  7.2 41.4 %all-gather.9.cloned.1.call-start = ((), (), s32[]{:S(2)}) async-start(), calls=%async_computation.2 | async-start | bytes 1351680 | tf_op jit(solution)/shard_map/all_gather | solution.py:28
  14.0 21.6 %copy-start.9 = (s32[12]{0:T(128)S(1)}, s32[12]{0:T(128)}, u32[]{:S(2)}) copy-start(s32[12]{0:T(128)} %param.19) | copy-start | bytes 148
  19.1 65.6 %all-reduce.19.cloned.1.call-start = ((), (), s32[]{:S(2)}) async-start(), calls=%async_computation | async-start | bytes 540672 | tf_op jit(solution)/shard_map/psum | solution.py:27
  24.3 78.2 %copy-start.8 = (u32[32]{0:T(128)S(1)}, u32[32]{0:T(128)}, u32[]{:S(2)}) copy-start(u32[32]{0:T(128)} %constant.56) | copy-start | bytes 388
  24.3 79.5 %copy-start.7 = (u32[32]{0:T(128)S(1)}, u32[32]{0:T(128)}, u32[]{:S(2)}) copy-start(u32[32]{0:T(128)} %constant.60) | copy-start | bytes 388
  24.3 95.1 %copy-start.1 = (bf16[1024,512]{1,0:T(8,128)(2,1)S(1)}, bf16[1024,512]{1,0:T(8,128)(2,1)}, u32[]{:S(2)}) copy-start(bf16[1024,512]{1,0:T(8,128)(2,1)} %param.26) | copy-start | bytes 3145732
  24.3 95.1 %copy-start.3 = (f32[1024]{0:T(1024)S(1)}, f32[1024]{0:T(1024)}, u32[]{:S(2)}) copy-start(f32[1024]{0:T(1024)} %param.25) | copy-start | bytes 12292
  24.3 95.4 %copy-start.2 = (bf16[1024,512]{1,0:T(8,128)(2,1)S(1)}, bf16[1024,512]{1,0:T(8,128)(2,1)}, u32[]{:S(2)}) copy-start(bf16[1024,512]{1,0:T(8,128)(2,1)} %param.27) | copy-start | bytes 3145732
  24.3 195.2 %all-gather.11.cloned.1.call-start = ((), (), s32[]{:S(2)}) async-start(), calls=%async_computation.3 | async-start | bytes 1351680 | tf_op jit(solution)/shard_map/all_gather | solution.py:28
  89.2 59.5 %copy-start.6 = (f32[512]{0:T(512)S(1)}, f32[512]{0:T(512)}, u32[]{:S(2)}) copy-start(f32[512]{0:T(512)} %param.31) | copy-start | bytes 6148
  98.3 7.4 %collective-permute-start = (bf16[12,1024]{1,0:T(8,128)(2,1)S(1)}, bf16[12,1024]{1,0:T(8,128)(2,1)S(1)}, u32[]{:S(2)}, u32[]{:S(2)}) collective-permute-start(bf16[12,1024]{1,0:T(8,128)(2,1)S(1)} %slice.20), channel_id=1, source_target_pairs={{0,1},{1,2},{2,3},{4,5},{5,6},{6,7},{8,9},{9,10},{10,11},{12,13},{... | collective-permute-start | bytes 73736
  119.7 66.5 %copy-start.5 = (f32[1024]{0:T(1024)S(1)}, f32[1024]{0:T(1024)}, u32[]{:S(2)}) copy-start(f32[1024]{0:T(1024)} %param.32) | copy-start | bytes 12292
  133.6 8.9 %collective-permute-start.3 = (bf16[12,512]{1,0:T(8,128)(2,1)S(1)}, bf16[12,512]{1,0:T(8,128)(2,1)S(1)}, u32[]{:S(2)}, u32[]{:S(2)}) collective-permute-start(bf16[12,512]{1,0:T(8,128)(2,1)S(1)} %slice.23), channel_id=1, source_target_pairs={{0,4},{4,8},{8,12},{1,5},{5,9},{9,13},{2,6},{6,10},{10,14},{3,7},{... | collective-permute-start | bytes 36872
  135.2 7.4 %collective-permute-start.2 = (bf16[12,512]{1,0:T(8,128)(2,1)S(1)}, bf16[12,512]{1,0:T(8,128)(2,1)S(1)}, u32[]{:S(2)}, u32[]{:S(2)}) collective-permute-start(bf16[12,512]{1,0:T(8,128)(2,1)S(1)} %slice.22), channel_id=1, source_target_pairs={{0,4},{4,8},{8,12},{1,5},{5,9},{9,13},{2,6},{6,10},{10,14},{3,7},{... | collective-permute-start | bytes 36872
  137.2 5.6 %collective-permute-start.4 = (bf16[12,512]{1,0:T(8,128)(2,1)S(1)}, bf16[12,512]{1,0:T(8,128)(2,1)S(1)}, u32[]{:S(2)}, u32[]{:S(2)}) collective-permute-start(bf16[12,512]{1,0:T(8,128)(2,1)S(1)} %slice.24), channel_id=1, source_target_pairs={{0,4},{4,8},{8,12},{1,5},{5,9},{9,13},{2,6},{6,10},{10,14},{3,7},{... | collective-permute-start | bytes 36872
  140.4 2.8 collective-permute-start.1
  174.5 5.2 %collective-permute-start.5 = (bf16[12,1024]{1,0:T(8,128)(2,1)S(1)}, bf16[12,1024]{1,0:T(8,128)(2,1)S(1)}, u32[]{:S(2)}, u32[]{:S(2)}) collective-permute-start(bf16[12,1024]{1,0:T(8,128)(2,1)S(1)} %slice.25), channel_id=1, source_target_pairs={{0,1},{1,2},{2,3},{4,5},{5,6},{6,7},{8,9},{9,10},{10,11},{12,13},{... | collective-permute-start | bytes 73736
  191.3 64.0 %all-reduce.21.cloned.1.call-start = ((), (), s32[]{:S(2)}) async-start(), calls=%async_computation.1 | async-start | bytes 540672 | tf_op jit(solution)/shard_map/psum | solution.py:27
  267.6 7.8 %collective-permute-start.6 = (bf16[12,1024]{1,0:T(8,128)(2,1)S(1)}, bf16[12,1024]{1,0:T(8,128)(2,1)S(1)}, u32[]{:S(2)}, u32[]{:S(2)}) collective-permute-start(bf16[12,1024]{1,0:T(8,128)(2,1)S(1)} %slice.26), channel_id=1, source_target_pairs={{0,1},{1,2},{2,3},{4,5},{5,6},{6,7},{8,9},{9,10},{10,11},{12,13},{... | collective-permute-start | bytes 73736
Sparse Core Ops, SparseCore 0:
  19.2 29.2 all-gather.8
  50.9 33.7 all-reduce.18
  191.4 28.0 all-gather.10
  221.7 33.5 all-reduce.20
